TPU v7x, 512 devices: a whole 4x8x8 slice. The times are simulated.
512 devices in a mesh: sp: 64 (over z, y), tp: 8 (over x, core).
Axes of the slice: x: 4, y: 8, z: 8, core: 2. Of those that a mesh axis runs over, the one named last changes fastest.
Arguments:
- residual: bfloat16 [8192, 2048], P(('sp', 'tp')), may hold values from -6 to 6
- q_small: bfloat16 [8192, 1024], P('sp', 'tp'), may hold values from -6 to 6
- k_small: bfloat16 [8192, 1024], P('sp', 'tp'), may hold values from -6 to 6
- v_small: bfloat16 [8192, 1024], P('sp', 'tp'), may hold values from -6 to 6
- q_large: bfloat16 [8192, 1024], P('sp', 'tp'), may hold values from -6 to 6
- k_large: bfloat16 [8192, 1024], P('sp', 'tp'), may hold values from -6 to 6
- v_large: bfloat16 [8192, 1024], P('sp', 'tp'), may hold values from -6 to 6
- forget_small: float32 [8192, 16], P('sp', 'tp'), may hold values from 0 to 20
- forget_large: float32 [8192, 8], P('sp', 'tp'), may hold values from 0 to 20
- w_out_small: bfloat16 [1024, 2048], P('tp'), may hold values from -0.125 to 0.125
- w_out_large: bfloat16 [1024, 2048], P('tp'), may hold values from -0.125 to 0.125
- norm_gain: float32 [2048], replicated, may hold values from 0.1 to 1.9
- w_gate: bfloat16 [2048, 4096], P('sp', 'tp'), may hold values from -0.125 to 0.125
- w_up: bfloat16 [2048, 4096], P('sp', 'tp'), may hold values from -0.125 to 0.125
- conv_gate: float32 [3, 4096], P(None, 'tp'), may hold values from -3 to 3
- conv_up: float32 [3, 4096], P(None, 'tp'), may hold values from -3 to 3
- w_down: bfloat16 [4096, 2048], P('tp', 'sp'), may hold values from -0.09375 to 0.09375
Outputs:
- mixed: bfloat16 [8192, 2048], P(('sp', 'tp'))
All inputs are finite; a program needn't handle non-finite values.
Results may differ from a plain program's by a relative error of at most 0.015.
Values may be sent and summed in bfloat16 or wider, within the bound.
A program may use at most 64 MiB of HBM per device.

v0:
```python
import jax
import jax.numpy as jnp
from jax import lax
from jax.sharding import PartitionSpec as P

EPS = 1e-06
NEG = -1e30


def rows_first(arrays, axis, dims):
    turned = [jnp.moveaxis(a, dim, 0) for a, dim in zip(arrays, dims)]
    widths = [t[0].size for t in turned]
    both = jnp.concatenate([t.reshape(-1, w) for t, w in zip(turned, widths)], axis=1)
    whole = lax.all_gather(both, axis, axis=0, tiled=True)
    parts = jnp.split(whole, [sum(widths[:k]) for k in range(1, len(widths))], axis=1)
    return tuple(
        (
            jnp.moveaxis(b.reshape(-1, *t.shape[1:]), 0, dim)
            for b, t, dim in zip(parts, turned, dims)
        )
    )


def in_one_piece(arrays, axis, dim, along):
    widths = [a.shape[along] for a in arrays]
    both = jnp.concatenate(arrays, axis=along)
    whole = lax.all_gather(both, axis, axis=dim, tiled=True)
    return tuple(jnp.split(whole, [sum(widths[:k]) for k in range(1, len(widths))], axis=along))


def in_blocks(array, dim, size):
    before, after = (array.shape[:dim], array.shape[dim + 1 :])
    return jnp.moveaxis(array.reshape(*before, size, -1, *after), dim, 0)


def sent_and_summed(array, axis, dim):
    size = lax.axis_size(axis)
    parts = lax.all_to_all(in_blocks(array, dim, size), axis, 0, 0, tiled=True)
    return jnp.sum(parts.astype(jnp.float32), axis=0)


def sent_to_all(array, axis):
    size = lax.axis_size(axis)
    return lax.all_to_all(
        jnp.broadcast_to(array[None], (size, *array.shape)), axis, 0, 0, tiled=True
    )


def in_order(parts, dim):
    parts = jnp.moveaxis(parts, 0, dim)
    lengths = parts.shape
    return parts.reshape(*lengths[:dim], lengths[dim] * lengths[dim + 1], *lengths[dim + 2 :])


def gather_directly(array, axis, dim):
    parts = sent_to_all(array, axis)
    return in_order(parts, dim)


def from_behind(block, axis, distance):
    devices = range(lax.axis_size(axis))
    route = [(i - distance, i) for i in devices if i - distance in devices]
    return lax.ppermute(block, axis, route)


def globalize(part, rows):
    heads = part.shape[1]
    blocks = part.reshape(-1, rows, heads)
    totals = blocks[:, -1, :]
    before = jnp.cumsum(totals, axis=0) - totals
    return (blocks + before[:, None, :]).reshape(part.shape)


def attend(carry, keys, values, queries, cum_own, cum_every, qpos):
    top, denom, accum = carry
    count = keys.shape[0]
    heads = queries.shape[1]
    size = queries.shape[2]
    keys = keys.reshape(count, heads, size)
    values = values.reshape(count, heads, size)
    kpos = jnp.arange(count, dtype=jnp.int32)
    scores = jnp.einsum(
        "qhd,khd->qhk", queries, keys, preferred_element_type=jnp.float32
    ) * size ** (-0.5)
    scores = scores + cum_own[:, :, None] - cum_every.T[None, :, :]
    keep = (kpos[None, :] <= qpos[:, None])[:, None, :]
    scores = jnp.where(keep, scores, NEG)
    new_top = jnp.maximum(top, jnp.max(scores, axis=-1))
    weights = jnp.where(keep, jnp.exp(scores - new_top[:, :, None]), 0.0)
    denom = jnp.sum(weights, axis=-1)
    accum = jnp.einsum(
        "qhk,khd->qhd", weights.astype(jnp.bfloat16), values, preferred_element_type=jnp.float32
    )
    return (new_top, denom, accum)


def finish(carry):
    top, denom, accum = carry
    attended = accum / denom[:, :, None]
    normed = attended * lax.rsqrt(jnp.mean(attended * attended, axis=-1, keepdims=True) + EPS)
    return normed.astype(jnp.bfloat16).reshape(attended.shape[0], -1)


def empty_carry(rows, heads, size):
    return (
        jnp.full((rows, heads), NEG, jnp.float32),
        jnp.zeros((rows, heads), jnp.float32),
        jnp.zeros((rows, heads, size), jnp.float32),
    )


def body(
    residual,
    q_small,
    k_small,
    v_small,
    q_large,
    k_large,
    v_large,
    forget_small,
    forget_large,
    w_out_small,
    w_out_large,
    norm_gain,
    w_gate,
    w_up,
    conv_gate,
    conv_up,
    w_down,
):
    rows = q_small.shape[0]
    offset = lax.axis_index("sp") * rows
    qpos = offset + jnp.arange(rows, dtype=jnp.int32)
    gathered = rows_first((w_gate, w_up, w_down), "sp", (0, 0, 1))
    local_small = jnp.cumsum(jax.nn.log_sigmoid(forget_small), axis=0)
    local_large = jnp.cumsum(jax.nn.log_sigmoid(forget_large), axis=0)
    part_small, part_large = in_one_piece((local_small, local_large), "sp", 0, 1)
    every_small = globalize(part_small, rows)
    every_large = globalize(part_large, rows)
    cum_small = lax.dynamic_slice_in_dim(every_small, offset, rows, 0)
    cum_large = lax.dynamic_slice_in_dim(every_large, offset, rows, 0)
    heads_small = forget_small.shape[1]
    heads_large = forget_large.shape[1]
    queries_small = q_small.reshape(rows, heads_small, -1)
    queries_large = q_large.reshape(rows, heads_large, -1)
    start_carry = (
        empty_carry(rows, heads_small, queries_small.shape[2]),
        empty_carry(rows, heads_large, queries_large.shape[2]),
    )
    keys_s, values_s, keys_l, values_l = in_one_piece(
        (k_small, v_small, k_large, v_large), "sp", 0, 1
    )
    small = attend(start_carry[0], keys_s, values_s, queries_small, cum_small, every_small, qpos)
    large = attend(start_carry[1], keys_l, values_l, queries_large, cum_large, every_large, qpos)
    normed_small = finish(small)
    normed_large = finish(large)
    first_part = jnp.dot(normed_small, w_out_small, preferred_element_type=jnp.float32)
    projected = sent_and_summed(
        (
            first_part + jnp.dot(normed_large, w_out_large, preferred_element_type=jnp.float32)
        ).astype(jnp.bfloat16),
        "tp",
        0,
    )
    first = residual.astype(jnp.float32) + projected
    normal = (
        first * lax.rsqrt(jnp.mean(first * first, axis=-1, keepdims=True) + EPS) * norm_gain
    ).astype(jnp.bfloat16)
    gate_full, up_full, down_full = gathered
    piece = gather_directly(normal, "tp", 0)
    gate_part = jnp.dot(piece, gate_full, preferred_element_type=jnp.float32).astype(jnp.bfloat16)
    up_part = jnp.dot(piece, up_full, preferred_element_type=jnp.float32).astype(jnp.bfloat16)
    both = jnp.concatenate([gate_part, up_part], axis=1)
    width = both.shape[0]
    rim = from_behind(both[width - 2 :], "sp", 1)
    extended = jnp.concatenate([rim, both], axis=0).astype(jnp.float32)
    taps = jnp.concatenate([conv_gate, conv_up], axis=1)
    conv = (
        taps[0] * extended[0:width]
        + taps[1] * extended[1 : width + 1]
        + taps[2] * extended[2 : width + 2]
    )
    half = gate_full.shape[1]
    hidden = (jax.nn.silu(conv[:, :half]) * conv[:, half:]).astype(jnp.bfloat16)
    mixed = first + sent_and_summed(
        jnp.dot(hidden, down_full, preferred_element_type=jnp.float32).astype(jnp.bfloat16), "tp", 0
    )
    return mixed.astype(jnp.bfloat16)


def solution(mesh):
    placed = (
        P(("sp", "tp"), None),
        P("sp", "tp"),
        P("sp", "tp"),
        P("sp", "tp"),
        P("sp", "tp"),
        P("sp", "tp"),
        P("sp", "tp"),
        P("sp", "tp"),
        P("sp", "tp"),
        P("tp", None),
        P("tp", None),
        P(),
        P("sp", "tp"),
        P("sp", "tp"),
        P(None, "tp"),
        P(None, "tp"),
        P("tp", "sp"),
    )
    return jax.shard_map(
        body, mesh=mesh, in_specs=placed, out_specs=P(("sp", "tp"), None), check_vma=False
    )
```

profile of v0, /device:TPU:64, one launch (start us, length us, event | category | flops | bytes accessed | tf_op | source)
XLA Modules:
  0.0 240.2 jit_solution(16217018536142575278)
XLA Ops:
  6.5 1.5 pad_maximum_fusion
  8.2 1.4 pad_maximum_fusion.1
  11.7 54.8 %all_gather.10 = f32[8192,3]{0,1:T(4,128)S(1)} all-gather(f32[128,3]{0,1:T(4,128)S(1)} %pad_maximum_fusion.3), channel_id=1, replica_groups=mesh['sp'=64,'tp'=8] {'sp'}, dimensions={0}, use_global_device_ids=true | all-gather | bytes 99840 | tf_op jit(solution)/shard_map/all_gather | solution.py:27
  67.3 2.7 %copy.48 = f32[8192,2]{1,0:T(8,128)} copy(f32[8192,2]{0,1:T(2,128)S(1)} %split.38) | data formatting | bytes 131072 | tf_op jit(solution)/shard_map/split | solution.py:28
  70.0 1.3 reduce-window_subtract_fusion.1
  71.8 1.7 iota_compare_fusion.1
  73.5 38.8 %all-gather.3.cloned.1.call-done = bf16[8192,512]{1,0:T(8,128)(2,1)} async-done(((bf16[128,512]{1,0:T(8,128)(2,1)}), bf16[8192,512]{1,0:T(8,128)(2,1)}) %all-gather.3.cloned.1.call-update) | async-done | bytes 8388624 | tf_op jit(solution)/shard_map/all_gather | solution.py:27
  112.3 3.9 %fusion.70 = (bf16[8192,128]{1,0:T(8,128)(2,1)}, bf16[8192,128]{1,0:T(8,128)(2,1)S(1)}) fusion(bf16[8192,512]{1,0:T(8,128)(2,1)} %all-gather.3.cloned.1.call-done), kind=kLoop, calls=%fused_computation.95 | loop fusion | bytes 8388608 | tf_op jit(solution)/shard_map/split | solution.py:28
  116.2 4.1 %copy.42 = bf16[8192,128]{0,1:T(8,128)(2,1)} copy(bf16[8192,128]{1,0:T(8,128)(2,1)} %get-tuple-element.5) | data formatting | bytes 4194304 | tf_op jit(solution)/shard_map/split | solution.py:28
  120.2 2.9 %copy.41 = bf16[8192,128]{0,1:T(8,128)(2,1)} copy(bf16[8192,128]{1,0:T(8,128)(2,1)S(1)} %get-tuple-element.6) | data formatting | bytes 4194304 | tf_op jit(solution)/shard_map/split | solution.py:28
  123.2 3.5 %fusion.74 = (f32[128]{0:T(128)S(1)}, f32[128,1,8192]{0,2,1:T(8,128)S(1)}) fusion(f32[8192]{0:T(1024)S(1)} %bitcast_add_fusion.1, f32[128]{0:T(128)S(1)} %fusion.65, bf16[128,128]{1,0:T(8,128)(2,1)S(1)} %copy-done.10, bf16[8192,512]{1,0:T(8,128)(2,1)} %all-gather.3.cloned.1.call-done, s32[128]{0:T(128)S(1)} %iota_add_fusion), kind=kOutput, calls=%fused_computation.99 | convolution fusion | flops 274726784 | bytes 6358528 | tf_op jit(solution)/shard_map/qhd,khd->qhk/dot_general | solution.py:82
  127.9 2.9 %multiply_reduce_fusion.1 = (f32[128]{0:T(128)S(1)}, f32[1,128,128]{2,1,0:T(8,128)S(1)}) fusion(f32[128]{0:T(128)S(1)} %fusion.16, f32[128,1,8192]{0,2,1:T(8,128)S(1)} %get-tuple-element.15, f32[128]{0:T(128)S(1)} %broadcast_maximum_fusion.1, s32[128]{0:T(128)S(1)} %iota_add_fusion, bf16[8192,512]{1,0:T(8,128)(2,1)} %all-gather.3.cloned.1.call-done), kind=kOutput, calls=%fused_computation.65 | convolution fusion | flops 272678784 | bytes 6359040 | tf_op jit(solution)/shard_map/qhk,khd->qhd/dot_general | solution.py:91
  130.8 3.6 %fusion.72 = (f32[128,2]{0,1:T(2,128)S(1)}, f32[128,2,8192]{0,2,1:T(8,128)S(1)}) fusion(f32[2,8192]{1,0:T(2,128)S(1)} %bitcast.93, f32[128,2]{0,1:T(2,128)S(1)} %constant_dynamic-slice_fusion.2, bf16[8192,2,64]{0,2,1:T(8,128)(2,1)S(1)} %bitcast.85, bf16[128,2,64]{0,2,1:T(8,128)(2,1)S(1)} %bitcast.95, pred[128,8192]{0,1:T(8,128)(4,1)S(1)} %copy-done.1), kind=kOutput, calls=%fused_computation.97 | convolution fusion | flops 278920960 | bytes 11634688 | tf_op jit(solution)/shard_map/qhd,khd->qhk/dot_general | solution.py:82
  134.5 1.7 fusion.9
  136.2 2.1 multiply_reduce_fusion.2
  139.1 14.4 %all_to_all.15 = bf16[8,16,2048]{2,1,0:T(8,128)(2,1)S(1)} all-to-all(bf16[8,16,2048]{2,1,0:T(8,128)(2,1)S(1)} %bitcast.83), channel_id=1, replica_groups=mesh['sp'=64,'tp'=8] {'tp'}, dimensions={0} | all-to-all | bytes 1048576 | tf_op jit(solution)/shard_map/all_to_all | solution.py:38
  154.7 3.5 %all-to-all-start.1 = ((bf16[8,16,2048]{2,1,0:T(8,128)(2,1)}), bf16[8,16,2048]{2,1,0:T(8,128)(2,1)S(1)}, u32[]{:S(2)}, u32[]{:S(2)}) async-start(bf16[8,16,2048]{2,1,0:T(8,128)(2,1)} %broadcast_in_dim.63), calls=%async_computation.1 | async-start | bytes 1048576 | tf_op jit(solution)/shard_map/all_to_all | solution.py:44
  158.2 45.6 %all-gather.5.cloned.1.call-done = bf16[2048,1536]{1,0:T(8,128)(2,1)} async-done(((bf16[32,1536]{1,0:T(8,128)(2,1)}), bf16[2048,1536]{1,0:T(8,128)(2,1)}) %all-gather.5.cloned.1.call-update) | async-done | bytes 6291472 | tf_op jit(solution)/shard_map/all_gather | solution.py:14
  203.9 2.0 fusion.32
  205.9 2.0 fusion.35
  208.0 3.1 %collective-permute-start = (bf16[2,1024]{1,0:T(2,128)(2,1)S(1)}, bf16[2,1024]{1,0:T(2,128)(2,1)S(1)}, u32[]{:S(2)}, u32[]{:S(2)}) collective-permute-start(bf16[2,1024]{1,0:T(2,128)(2,1)S(1)} %pad_maximum_fusion.2), channel_id=1, source_target_pairs={{0,8},{8,16},{16,24},{24,32},{32,40},{40,48},{48,56},{56,64},{64,7... | collective-permute-start | bytes 12296 | tf_op jit(solution)/shard_map/ppermute | solution.py:63
  211.0 4.5 %collective-permute-done = bf16[2,1024]{1,0:T(2,128)(2,1)S(1)} collective-permute-done((bf16[2,1024]{1,0:T(2,128)(2,1)S(1)}, bf16[2,1024]{1,0:T(2,128)(2,1)S(1)}, u32[]{:S(2)}, u32[]{:S(2)}) %collective-permute-start) | collective-permute-done | bytes 4128 | tf_op jit(solution)/shard_map/ppermute | solution.py:63
  215.8 2.4 %convolution_convert_fusion = bf16[128,2048]{1,0:T(8,128)(2,1)S(1)} fusion(bf16[2048,1536]{1,0:T(8,128)(2,1)} %all-gather.5.cloned.1.call-done, f32[128,1024]{1,0:T(8,128)S(1)} %fusion.54), kind=kOutput, calls=%fused_computation.25 | convolution fusion | flops 269090816 | bytes 3145728 | tf_op jit(solution)/shard_map/dot_general | solution.py:186
  218.2 14.4 %all_to_all.16 = bf16[8,16,2048]{2,1,0:T(8,128)(2,1)S(1)} all-to-all(bf16[8,16,2048]{2,1,0:T(8,128)(2,1)S(1)} %bitcast.88), channel_id=1, replica_groups=mesh['sp'=64,'tp'=8] {'tp'}, dimensions={0} | all-to-all | bytes 1048576 | tf_op jit(solution)/shard_map/all_to_all | solution.py:38
  (70 shorter events, 7.4 us)
Async XLA Ops:
  6.5 131.9 %copy-start = (bf16[128,2048]{1,0:T(8,128)(2,1)S(1)}, bf16[128,2048]{1,0:T(8,128)(2,1)}, u32[]{:S(2)}) copy-start(bf16[128,2048]{1,0:T(8,128)(2,1)} %param.26) | copy-start | bytes 1572868
  6.5 64.9 %copy-start.6 = (bf16[128,128]{1,0:T(8,128)(2,1)S(1)}, bf16[128,128]{1,0:T(8,128)(2,1)}, u32[]{:S(2)}) copy-start(bf16[128,128]{1,0:T(8,128)(2,1)} %param.18) | copy-start | bytes 98308
  6.5 105.8 %all-gather.3.cloned.1.call-start = ((), (), s32[]{:S(2)}) async-start(), calls=%async_computation.3 | async-start | bytes 8519680 | tf_op jit(solution)/shard_map/all_gather | solution.py:27
  8.1 195.8 %all-gather.5.cloned.1.call-start = ((), (), s32[]{:S(2)}) async-start(), calls=%async_computation.4 | async-start | bytes 6389760 | tf_op jit(solution)/shard_map/all_gather | solution.py:14
  116.2 7.0 %copy-start.10 = (bf16[128,128]{1,0:T(8,128)(2,1)S(1)}, bf16[128,128]{1,0:T(8,128)(2,1)}, u32[]{:S(2)}) copy-start(bf16[128,128]{1,0:T(8,128)(2,1)} %param.21) | copy-start | bytes 98308
  127.8 3.0 %copy-start.1 = (pred[128,8192]{0,1:T(8,128)(4,1)S(1)}, pred[128,8192]{0,1:T(8,128)(4,1)}, u32[]{:S(2)}) copy-start(pred[128,8192]{0,1:T(8,128)(4,1)} %iota_compare_fusion.1) | copy-start | bytes 3145732
  127.8 3.0 %copy-start.3 = (bf16[8192,128]{0,1:T(8,128)(2,1)S(1)}, bf16[8192,128]{0,1:T(8,128)(2,1)}, u32[]{:S(2)}) copy-start(bf16[8192,128]{0,1:T(8,128)(2,1)} %copy.42) | copy-start | bytes 6291460
  134.5 1.7 copy-start.2
  136.2 2.6 %copy-start.5 = (bf16[128,2048]{1,0:T(8,128)(2,1)S(1)}, bf16[128,2048]{1,0:T(8,128)(2,1)}, u32[]{:S(2)}) copy-start(bf16[128,2048]{1,0:T(8,128)(2,1)} %param.27) | copy-start | bytes 1572868
  138.3 15.2 %copy-start.4 = (bf16[16,2048]{1,0:T(8,128)(2,1)S(1)}, bf16[16,2048]{1,0:T(8,128)(2,1)}, u32[]{:S(2)}) copy-start(bf16[16,2048]{1,0:T(8,128)(2,1)} %param.17) | copy-start | bytes 196612
  138.3 15.4 %copy-start.7 = (f32[2048]{0:T(1024)S(1)}, f32[2048]{0:T(1024)}, u32[]{:S(2)}) copy-start(f32[2048]{0:T(1024)} %param.28) | copy-start | bytes 24580
  138.4 19.8 %copy-start.8 = (f32[3,512]{1,0:T(4,128)S(1)}, f32[3,512]{1,0:T(4,128)}, u32[]{:S(2)}) copy-start(f32[3,512]{1,0:T(4,128)} %param.31) | copy-start | bytes 18436
  138.4 19.8 %copy-start.9 = (f32[3,512]{1,0:T(4,128)S(1)}, f32[3,512]{1,0:T(4,128)}, u32[]{:S(2)}) copy-start(f32[3,512]{1,0:T(4,128)} %param.32) | copy-start | bytes 18436
  154.7 49.2 %all-to-all-start.1 = ((bf16[8,16,2048]{2,1,0:T(8,128)(2,1)}), bf16[8,16,2048]{2,1,0:T(8,128)(2,1)S(1)}, u32[]{:S(2)}, u32[]{:S(2)}) async-start(bf16[8,16,2048]{2,1,0:T(8,128)(2,1)} %broadcast_in_dim.63), calls=%async_computation.1 | async-start | bytes 1048576 | tf_op jit(solution)/shard_map/all_to_all | solution.py:44
  208.0 7.6 %collective-permute-start = (bf16[2,1024]{1,0:T(2,128)(2,1)S(1)}, bf16[2,1024]{1,0:T(2,128)(2,1)S(1)}, u32[]{:S(2)}, u32[]{:S(2)}) collective-permute-start(bf16[2,1024]{1,0:T(2,128)(2,1)S(1)} %pad_maximum_fusion.2), channel_id=1, source_target_pairs={{0,8},{8,16},{16,24},{24,32},{32,40},{40,48},{48,56},{56,64},{64,7... | collective-permute-start | bytes 12296 | tf_op jit(solution)/shard_map/ppermute | solution.py:63
Sparse Core Ops, SparseCore 0:
  10.4 101.8 all-gather.2
  115.3 88.5 all-gather.4
where the time goes:
time: 241 us; the launch traced here: 240 us
  waiting for transfers between devices  89 us (37%)
  blocking collectives  83.6 us (35%)
  matrix products  19.4 us (8%)
  local copies, waits for them, and re-layouts  15.3 us (6%)
  between operations  13.7 us (6%)
  other arithmetic  12.5 us (5%)
  starting transfers between devices  6.59 us (3%)
    all_gather x1, blocking collectives, in_one_piece(): whole = lax.all_gather(both, axis, axis=dim, tiled=True)  54.8 us
    all_gather x1, waiting for transfers between devices, rows_first(): whole = lax.all_gather(both, axis, axis=0, tiled=True)  45.6 us
    all_gather x1, waiting for transfers between devices, in_one_piece(): whole = lax.all_gather(both, axis, axis=dim, tiled=True)  38.8 us
    all_to_all x2, blocking collectives, sent_and_summed(): parts = lax.all_to_all(in_blocks(array, dim, size), axis, 0, 0, tiled=True)  28.8 us
    split x6, local copies, waits for them, and re-layouts, in_one_piece(): jnp.split(whole, [sum(widths[:k]) for k in range(1, len(widths))], axis=a...  13.6 us
    dot_general x2, matrix products, attend(): jnp.einsum('qhd,khd->qhk', queries, keys, preferred_element_type=jnp.floa...  7.16 us
    dot_general x2, matrix products, attend(): jnp.einsum('qhk,khd->qhd', weights.astype(jnp.bfloat16), values, preferre...  5.09 us
  transfers between devices with their start and end apart: 4, of which 3 were waited for; matrix products, arithmetic and copies ran while one was open for 16% of the time, Pallas kernels for 0%

commit v1 on v0

--- a/solution.py
+++ b/solution.py
@@ -11,7 +11,8 @@
     turned = [jnp.moveaxis(a, dim, 0) for a, dim in zip(arrays, dims)]
     widths = [t[0].size for t in turned]
     both = jnp.concatenate([t.reshape(-1, w) for t, w in zip(turned, widths)], axis=1)
-    whole = lax.all_gather(both, axis, axis=0, tiled=True)
+    repeated = jnp.stack([both] * lax.axis_size(axis))
+    whole = jnp.concatenate(lax.all_to_all(repeated, axis, 0, 0), axis=0)
     parts = jnp.split(whole, [sum(widths[:k]) for k in range(1, len(widths))], axis=1)
     return tuple(
         (

time: 241 us -> 429 us (1.78)
  the two profiles are of different devices: /device:TPU:64 before, /device:TPU:40 now
where the time goes in v1:
time: 429 us; the launch traced here: 428 us
  waiting for transfers between devices  263 us (61%)
  blocking collectives  67.6 us (16%)
  starting transfers between devices  27.4 us (6%)
  matrix products  23.8 us (6%)
  local copies, waits for them, and re-layouts  18.6 us (4%)
  between operations  13.7 us (3%)
  other arithmetic  13.5 us (3%)
    all_to_all x1, waiting for transfers between devices, rows_first(): whole = jnp.concatenate(lax.all_to_all(repeated, axis, 0, 0), axis=0)  198 us
    all_gather x1, blocking collectives, in_one_piece(): whole = lax.all_gather(both, axis, axis=dim, tiled=True)  54.9 us
    all_gather x1, waiting for transfers between devices, in_one_piece(): whole = lax.all_gather(both, axis, axis=dim, tiled=True)  40.9 us
    all_to_all x1, blocking collectives, sent_and_summed(): parts = lax.all_to_all(in_blocks(array, dim, size), axis, 0, 0, tiled=True)  12.8 us
    split x6, local copies, waits for them, and re-layouts, in_one_piece(): jnp.split(whole, [sum(widths[:k]) for k in range(1, len(widths))], axis=a...  11.4 us
    dot_general x2, matrix products, attend(): jnp.einsum('qhd,khd->qhk', queries, keys, preferred_element_type=jnp.floa...  11 us
    all_to_all x1, starting transfers between devices, sent_to_all(): lax.all_to_all(jnp.broadcast_to(array[None], (size, *array.shape)), axis,...  10.9 us
    all_to_all x1, starting transfers between devices, rows_first(): whole = jnp.concatenate(lax.all_to_all(repeated, axis, 0, 0), axis=0)  10.4 us
  transfers between devices with their start and end apart: 5, of which 5 were waited for; matrix products, arithmetic and copies ran while one was open for 2% of the time, Pallas kernels for 0%

profile of v1, /device:TPU:40, one launch (start us, length us, event | category | flops | bytes accessed | tf_op | source)
XLA Modules:
  0.0 427.8 jit_solution(12771863282821746170)
XLA Ops:
  10.2 54.9 %all_gather.7 = f32[8192,3]{0,1:T(4,128)S(1)} all-gather(f32[128,3]{0,1:T(4,128)S(1)} %pad_maximum_fusion.3), channel_id=1, replica_groups=mesh['sp'=64,'tp'=8] {'sp'}, dimensions={0}, use_global_device_ids=true | all-gather | bytes 99840 | tf_op jit(solution)/shard_map/all_gather | solution.py:28
  66.1 2.6 copy.48
  72.9 40.9 %all-gather.2.cloned.1.call-done = bf16[8192,512]{1,0:T(8,128)(2,1)} async-done(((bf16[128,512]{1,0:T(8,128)(2,1)}), bf16[8192,512]{1,0:T(8,128)(2,1)}) %all-gather.2.cloned.1.call-update) | async-done | bytes 8388624 | tf_op jit(solution)/shard_map/all_gather | solution.py:28
  113.7 4.2 fusion.74
  120.9 4.1 copy.42
  125.0 3.4 fusion.16
  128.5 2.8 multiply_reduce_fusion.1
  131.2 3.0 copy.41
  134.2 6.8 %fusion.72 = (f32[128,2]{0,1:T(2,128)S(1)}, f32[128,2,8192]{0,2,1:T(8,128)S(1)}) fusion(f32[2,8192]{1,0:T(2,128)S(1)} %bitcast.93, f32[128,2]{0,1:T(2,128)S(1)} %constant_dynamic-slice_fusion.2, bf16[8192,2,64]{0,2,1:T(8,128)(2,1)} %bitcast.84, bf16[128,2,64]{0,2,1:T(8,128)(2,1)S(1)} %bitcast.95, pred[128,8192]{0,1:T(8,128)(4,1)} %iota_compare_fusion.1), kind=kOutput, calls=%fused_computation.97 | convolution fusion | flops 278920960 | bytes 11634688 | tf_op jit(solution)/shard_map/qhd,khd->qhk/dot_general | solution.py:83
  141.0 1.7 fusion.9
  142.7 2.1 multiply_reduce_fusion.2
  146.4 4.3 all-to-all-start
  150.7 10.3 %all-to-all-done = bf16[8,16,2048]{2,1,0:T(8,128)(2,1)S(1)} async-done(((bf16[8,16,2048]{2,1,0:T(8,128)(2,1)}), bf16[8,16,2048]{2,1,0:T(8,128)(2,1)S(1)}, u32[]{:S(2)}, u32[]{:S(2)}) %all-to-all-start) | async-done | bytes 524320 | tf_op jit(solution)/shard_map/all_to_all | solution.py:39
  161.0 3.4 stack.2
  164.4 10.4 %all-to-all-start.2 = ((bf16[64,32,1536]{2,1,0:T(8,128)(2,1)}), bf16[64,32,1536]{2,1,0:T(8,128)(2,1)}, u32[]{:S(2)}, u32[]{:S(2)}) async-start(bf16[64,32,1536]{2,1,0:T(8,128)(2,1)} %stack.2), calls=%async_computation.2 | async-start | bytes 12582912 | tf_op jit(solution)/shard_map/all_to_all | solution.py:15
  175.1 198.1 %all-to-all-done.2 = bf16[64,32,1536]{2,1,0:T(8,128)(2,1)} async-done(((bf16[64,32,1536]{2,1,0:T(8,128)(2,1)}), bf16[64,32,1536]{2,1,0:T(8,128)(2,1)}, u32[]{:S(2)}, u32[]{:S(2)}) %all-to-all-start.2) | async-done | bytes 6291488 | tf_op jit(solution)/shard_map/all_to_all | solution.py:15
  374.1 10.9 %all-to-all-start.1 = ((bf16[8,16,2048]{2,1,0:T(8,128)(2,1)}), bf16[8,16,2048]{2,1,0:T(8,128)(2,1)S(1)}, u32[]{:S(2)}, u32[]{:S(2)}) async-start(bf16[8,16,2048]{2,1,0:T(8,128)(2,1)} %broadcast_in_dim.63), calls=%async_computation.1 | async-start | bytes 1048576 | tf_op jit(solution)/shard_map/all_to_all | solution.py:45
  384.9 10.3 %all-to-all-done.1 = bf16[8,16,2048]{2,1,0:T(8,128)(2,1)S(1)} async-done(((bf16[8,16,2048]{2,1,0:T(8,128)(2,1)}), bf16[8,16,2048]{2,1,0:T(8,128)(2,1)S(1)}, u32[]{:S(2)}, u32[]{:S(2)}) %all-to-all-start.1) | async-done | bytes 524320 | tf_op jit(solution)/shard_map/all_to_all | solution.py:45
  395.2 2.0 fusion.35
  397.3 2.0 fusion.32
  399.3 1.9 collective-permute-start
  401.3 3.6 collective-permute-done
  405.1 2.4 convolution_convert_fusion
  407.5 12.8 %all_to_all.20 = bf16[8,16,2048]{2,1,0:T(8,128)(2,1)S(1)} all-to-all(bf16[8,16,2048]{2,1,0:T(8,128)(2,1)S(1)} %bitcast.88), channel_id=1, replica_groups=mesh['sp'=64,'tp'=8] {'tp'}, dimensions={0} | all-to-all | bytes 1048576 | tf_op jit(solution)/shard_map/all_to_all | solution.py:39
  (77 shorter events, 15.4 us)
Async XLA Ops:
  6.5 138.4 %copy-start = (bf16[128,2048]{1,0:T(8,128)(2,1)S(1)}, bf16[128,2048]{1,0:T(8,128)(2,1)}, u32[]{:S(2)}) copy-start(bf16[128,2048]{1,0:T(8,128)(2,1)} %param.26) | copy-start | bytes 1572868
  6.5 107.2 %copy-start.13 = (bf16[128,128]{1,0:T(8,128)(2,1)S(1)}, bf16[128,128]{1,0:T(8,128)(2,1)}, u32[]{:S(2)}) copy-start(bf16[128,128]{1,0:T(8,128)(2,1)} %param.21) | copy-start | bytes 98308
  6.5 107.2 %all-gather.2.cloned.1.call-start = ((), (), s32[]{:S(2)}) async-start(), calls=%async_computation.4 | async-start | bytes 8519680 | tf_op jit(solution)/shard_map/all_gather | solution.py:28
  113.7 5.6 %copy-start.3 = (bf16[8192,512]{1,0:T(8,128)(2,1)S(1)}, bf16[8192,512]{1,0:T(8,128)(2,1)}, u32[]{:S(2)}) copy-start(bf16[8192,512]{1,0:T(8,128)(2,1)} %all-gather.2.cloned.1.call-done) | copy-start | bytes 25165828
  125.0 3.4 copy-start.2
  134.2 6.8 %copy-start.1 = (pred[128,8192]{0,1:T(8,128)(4,1)S(1)}, pred[128,8192]{0,1:T(8,128)(4,1)}, u32[]{:S(2)}) copy-start(pred[128,8192]{0,1:T(8,128)(4,1)} %iota_compare_fusion.1) | copy-start | bytes 3145732
  141.0 1.7 copy-start.4
  142.7 2.6 copy-start.6
  144.9 5.8 %copy-start.7 = (bf16[512,32]{0,1:T(8,128)(2,1)S(1)}, bf16[512,32]{0,1:T(8,128)(2,1)}, u32[]{:S(2)}) copy-start(bf16[512,32]{0,1:T(8,128)(2,1)} %param.33) | copy-start | bytes 98308
  144.9 5.8 %copy-start.8 = (bf16[32,512]{1,0:T(8,128)(2,1)S(1)}, bf16[32,512]{1,0:T(8,128)(2,1)}, u32[]{:S(2)}) copy-start(bf16[32,512]{1,0:T(8,128)(2,1)} %param.30) | copy-start | bytes 98308
  144.9 5.8 %copy-start.9 = (bf16[32,512]{1,0:T(8,128)(2,1)S(1)}, bf16[32,512]{1,0:T(8,128)(2,1)}, u32[]{:S(2)}) copy-start(bf16[32,512]{1,0:T(8,128)(2,1)} %param.29) | copy-start | bytes 98308
  146.4 14.6 %all-to-all-start = ((bf16[8,16,2048]{2,1,0:T(8,128)(2,1)}), bf16[8,16,2048]{2,1,0:T(8,128)(2,1)S(1)}, u32[]{:S(2)}, u32[]{:S(2)}) async-start(bf16[8,16,2048]{2,1,0:T(8,128)(2,1)} %bitcast.20), calls=%async_computation | async-start | bytes 1048576 | tf_op jit(solution)/shard_map/all_to_all | solution.py:39
  164.4 10.5 %copy-start.5 = (bf16[16,2048]{1,0:T(8,128)(2,1)S(1)}, bf16[16,2048]{1,0:T(8,128)(2,1)}, u32[]{:S(2)}) copy-start(bf16[16,2048]{1,0:T(8,128)(2,1)} %param.17) | copy-start | bytes 196612
  164.4 10.6 %copy-start.10 = (f32[2048]{0:T(1024)S(1)}, f32[2048]{0:T(1024)}, u32[]{:S(2)}) copy-start(f32[2048]{0:T(1024)} %param.28) | copy-start | bytes 24580
  164.4 220.5 %copy-start.11 = (f32[3,512]{1,0:T(4,128)S(1)}, f32[3,512]{1,0:T(4,128)}, u32[]{:S(2)}) copy-start(f32[3,512]{1,0:T(4,128)} %param.31) | copy-start | bytes 18436
  164.4 220.5 %copy-start.12 = (f32[3,512]{1,0:T(4,128)S(1)}, f32[3,512]{1,0:T(4,128)}, u32[]{:S(2)}) copy-start(f32[3,512]{1,0:T(4,128)} %param.32) | copy-start | bytes 18436
  164.4 208.8 %all-to-all-start.2 = ((bf16[64,32,1536]{2,1,0:T(8,128)(2,1)}), bf16[64,32,1536]{2,1,0:T(8,128)(2,1)}, u32[]{:S(2)}, u32[]{:S(2)}) async-start(bf16[64,32,1536]{2,1,0:T(8,128)(2,1)} %stack.2), calls=%async_computation.2 | async-start | bytes 12582912 | tf_op jit(solution)/shard_map/all_to_all | solution.py:15
  374.1 21.2 %all-to-all-start.1 = ((bf16[8,16,2048]{2,1,0:T(8,128)(2,1)}), bf16[8,16,2048]{2,1,0:T(8,128)(2,1)S(1)}, u32[]{:S(2)}, u32[]{:S(2)}) async-start(bf16[8,16,2048]{2,1,0:T(8,128)(2,1)} %broadcast_in_dim.63), calls=%async_computation.1 | async-start | bytes 1048576 | tf_op jit(solution)/shard_map/all_to_all | solution.py:45
  399.3 5.5 %collective-permute-start = (bf16[2,1024]{1,0:T(2,128)(2,1)S(1)}, bf16[2,1024]{1,0:T(2,128)(2,1)S(1)}, u32[]{:S(2)}, u32[]{:S(2)}) collective-permute-start(bf16[2,1024]{1,0:T(2,128)(2,1)S(1)} %pad_maximum_fusion.2), channel_id=1, source_target_pairs={{0,8},{8,16},{16,24},{24,32},{32,40},{40,48},{48,56},{56,64},{64,7... | collective-permute-start | bytes 12296 | tf_op jit(solution)/shard_map/ppermute | solution.py:64
Sparse Core Ops, SparseCore 0:
  10.4 103.2 all-gather.1
